TPU v7x, 32 devices: a whole 2x2x4 slice. The times are simulated.
32 devices in a mesh: sp: 8 (over z, x), tp: 4 (over y, core).
Axes of the slice: x: 2, y: 2, z: 4, core: 2. Of those that a mesh axis runs over, the one named last changes fastest.
Arguments:
- query_logits: bfloat16 [4096, 4096], P('sp', 'tp'), may hold values from -6 to 6
- forget_logits: bfloat16 [4096, 4096], P('sp', 'tp'), may hold values from -6 to 6
- value_inputs: bfloat16 [4096, 4096], P('sp', 'tp'), may hold values from -16 to 16
- output_gate_logits: bfloat16 [4096, 4096], P('sp', 'tp'), may hold values from -6 to 6
- forget_floor_gap: float32 [4096], replicated, may hold values from 2.4414063e-05 to 0.1
- surge_log_decay: float32 [32, 4096], P('tp', 'sp'), may hold values from -0.7 to 0
- head_norm_gain: float32 [128], replicated, may hold values from 0.1 to 1.9
- output_matrix: bfloat16 [4096, 4096], P('sp', 'tp'), may hold values from -1.25 to 1.25
- branch_norm_gain: float32 [4096], replicated, may hold values from 0.1 to 1.9
- residual: bfloat16 [4096, 4096], P('sp', 'tp'), may hold values from -6 to 6
Outputs:
- output: bfloat16 [4096, 4096], P('sp', 'tp')
All inputs are finite; a program needn't handle non-finite values.
Results may differ from a plain program's by a relative error of at most 0.005.
Values may be sent and summed in bfloat16 or wider, within the bound.
No kernel may reach another device: no remote copies, remote signals or barrier semaphores. Data moves between devices by JAX's collectives and lax.ppermute only.
A program may use at most 128 MiB of HBM per device.

v0:
```python
import jax
import jax.numpy as jnp
from jax import lax
from jax.sharding import PartitionSpec as P

HEAD_DIM = 128
D = 4096
BLOCK_SPAN = 64
epsilon = 1e-06


def prefix(shard, axis, combine, identity):
    size, position = (lax.axis_size(axis), lax.axis_index(axis))
    everything = jax.tree.map(lambda part: lax.all_gather(part, axis), shard)
    start = jax.tree.map(
        lambda part, zero: jnp.broadcast_to(jnp.asarray(zero, part.dtype), part.shape),
        shard,
        identity,
    )

    def step(k, before):
        reached = k < position
        new = combine(before, jax.tree.map(lambda part: part[k], everything))
        return jax.tree.map(lambda a, b: jnp.where(reached, a, b), new, before)

    return lax.fori_loop(0, size, step, start)


def block_update(state, queries, keys_in, values_in, running):
    length = running.shape[1]
    middle = length // 2
    anchor = running[:, middle - 1 : middle, :]
    ending = running[:, -1:, :]
    causal = jnp.tril(jnp.ones((length, length), dtype=bool))
    highest = lax.Precision.HIGHEST
    inter = jnp.einsum("htd,hde->hte", queries * jnp.exp(running), state, precision=highest)
    scores = jnp.einsum(
        "htd,hsd->hts",
        queries * jnp.exp(running - anchor),
        keys_in * jnp.exp(anchor - running),
        precision=highest,
    )
    intra = jnp.einsum(
        "hts,hse->hte", jnp.where(causal[None], scores, 0.0), values_in, precision=highest
    )
    new_state = state * jnp.exp(ending[:, 0, :])[:, :, None] + jnp.einsum(
        "hsd,hse->hde", keys_in * jnp.exp(ending - running), values_in, precision=highest
    )
    return (new_state, inter + intra)


def head_gates(query_logits, forget_logits, value_inputs, gap):
    row_count = query_logits.shape[0]
    head_count = query_logits.shape[1] // HEAD_DIM

    def shaped(array):
        return array.astype(jnp.float32).reshape(row_count, head_count, HEAD_DIM)

    queries = jax.nn.silu(shaped(query_logits)) * HEAD_DIM ** (-0.5)
    keys_in = gap.reshape(head_count, HEAD_DIM) * jax.nn.sigmoid(-shaped(forget_logits))
    values_in = shaped(value_inputs)
    decay_factors = jnp.log1p(-keys_in)
    return (queries, keys_in, values_in, decay_factors)


def gated_norm(heads_out, output_gate_logits, head_norm_gain):
    mean_sq = jnp.mean(heads_out * heads_out, axis=-1, keepdims=True)
    gates = jax.nn.silu(output_gate_logits.astype(jnp.float32).reshape(heads_out.shape))
    normed = heads_out * lax.rsqrt(mean_sq + epsilon) * head_norm_gain * gates
    return normed.reshape(heads_out.shape[0], -1).astype(jnp.bfloat16)


def combine(earlier, later):
    return (earlier[0] * later[0], later[0][:, :, None] * earlier[1] + later[1])


def per_device(
    query_logits,
    forget_logits,
    value_inputs,
    output_gate_logits,
    forget_floor_gap,
    surge_log_decay,
    head_norm_gain,
    output_matrix,
    branch_norm_gain,
    residual,
):
    row_count = query_logits.shape[0]
    head_cols = query_logits.shape[1]
    head_count = head_cols // HEAD_DIM
    number_of_blocks = row_count // BLOCK_SPAN
    column = lax.axis_index("tp")
    whole_weight = lax.all_gather(output_matrix, "sp", axis=0, tiled=True)
    gap = lax.dynamic_slice_in_dim(forget_floor_gap, column * head_cols, head_cols)
    queries, keys_in, values_in, decay_factors = head_gates(
        query_logits, forget_logits, value_inputs, gap
    )
    decay_factors = decay_factors + jnp.transpose(surge_log_decay)[:, :, None]

    def to_blocks(array):
        return array.reshape(number_of_blocks, BLOCK_SPAN, head_count, HEAD_DIM).transpose(
            0, 2, 1, 3
        )

    queries = to_blocks(queries)
    running = jnp.cumsum(to_blocks(decay_factors), axis=2)

    def step_forward(state, input_tuple):
        return block_update(state, input_tuple[0], input_tuple[1], input_tuple[2], input_tuple[3])

    starting_state = jnp.zeros((head_count, HEAD_DIM, HEAD_DIM), jnp.float32)
    end_state, local_out = lax.scan(
        step_forward, starting_state, (queries, to_blocks(keys_in), to_blocks(values_in), running)
    )
    totals = running[:, :, -1, :]
    before = jnp.cumsum(totals, axis=0) - totals
    whole_decay = jnp.exp(jnp.sum(totals, axis=0))
    identity = (jnp.ones_like(whole_decay), jnp.zeros_like(end_state))
    unused_slot, carried = prefix((whole_decay, end_state), "sp", combine, identity)
    reach = queries * jnp.exp(running + before[:, :, None, :])
    heads_out = local_out + jnp.einsum(
        "nhtd,hde->nhte", reach, carried, precision=lax.Precision.HIGHEST
    )
    heads_out = heads_out.transpose(0, 2, 1, 3).reshape(row_count, head_count, HEAD_DIM)
    mixed_rows = gated_norm(heads_out, output_gate_logits, head_norm_gain)
    all_heads = lax.all_gather(mixed_rows, "tp", axis=1, tiled=True)
    projected = jnp.dot(all_heads, whole_weight, preferred_element_type=jnp.float32)
    branch = lax.optimization_barrier(projected.astype(jnp.bfloat16)).astype(jnp.float32)
    squares = lax.psum(jnp.sum(branch * branch, axis=1), "tp")
    scale = lax.rsqrt(squares / D + epsilon)
    out_cols = branch.shape[1]
    gain_part = lax.dynamic_slice_in_dim(branch_norm_gain, column * out_cols, out_cols)
    return (residual.astype(jnp.float32) + branch * scale[:, None] * gain_part).astype(jnp.bfloat16)


def solution(mesh):
    placed = (
        P("sp", "tp"),
        P("sp", "tp"),
        P("sp", "tp"),
        P("sp", "tp"),
        P(),
        P("tp", "sp"),
        P(),
        P("sp", "tp"),
        P(),
        P("sp", "tp"),
    )
    return jax.shard_map(
        per_device, mesh=mesh, in_specs=placed, out_specs=P("sp", "tp"), check_vma=False
    )
```

profile of v0, /device:TPU:0, one launch (start us, length us, event | category | flops | bytes accessed | tf_op | source)
XLA Modules:
  0.0 348.8 jit_solution(4762647425927424889)
XLA Ops:
  7.4 1.8 divide_bitcast_fusion
  9.2 1.8 copy.48
  13.2 1.5 bitcast_bitcast_fusion
  14.6 4.0 %fusion.36 = f32[8,8,64,128]{3,1,2,0:T(8,128)} fusion(f32[8,64,8]{2,1,0:T(8,128)S(1)} %bitcast.184, f32[8,128]{1,0:T(8,128)S(1)} %dynamic-slice_bitcast_fusion.1, f32[8,64,8,128]{3,2,1,0:T(8,128)} %bitcast.177), kind=kOutput, calls=%fused_computation.60 | output fusion | flops 34603008 | bytes 4214784 | tf_op jit(solution)/shard_map/jit(cumsum)/reduce_window_sum | solution.py:107
  18.6 2.5 fusion.34
  21.1 47.1 %while.27 = (s32[]{:T(128)}, f32[8,128,128]{2,1,0:T(8,128)S(1)}, f32[8,8,64,128]{3,2,0,1:T(8,128)}, f32[8,8,64,128]{3,1,2,0:T(8,128)}, f32[8,8,64,128]{3,1,2,0:T...) while((s32[]{:T(128)}, f32[8,128,128]{2,1,0:T(8,128)S(1)}, ...), condition=%wide.region_2.3_spmd.clone, body=%wide.region_1.2_spmd.clone.sunk | while | flops 303075328 | bytes 7647356 | solution.py:113
  21.1 1.1 constant_dynamic-slice_fusion.7
  22.2 1.1 constant_dynamic-slice_fusion.6
  24.1 1.2 convolution_add_fusion.3
  25.9 1.1 fusion.74
  28.1 1.1 constant_dynamic-slice_fusion.6
  29.9 1.2 convolution_add_fusion.3
  31.8 1.1 fusion.74
  34.0 1.1 constant_dynamic-slice_fusion.6
  35.8 1.2 convolution_add_fusion.3
  37.7 1.1 fusion.74
  39.9 1.1 constant_dynamic-slice_fusion.6
  41.7 1.2 convolution_add_fusion.3
  43.5 1.2 fusion.74
  45.8 1.1 constant_dynamic-slice_fusion.6
  47.6 1.2 convolution_add_fusion.3
  49.5 1.1 fusion.74
  53.5 1.2 convolution_add_fusion.3
  55.3 1.1 fusion.74
  59.3 1.2 convolution_add_fusion.3
  61.2 1.2 fusion.74
  65.2 1.2 convolution_add_fusion.3
  67.1 1.1 fusion.74
  69.9 33.1 %all-gather = f32[64,128]{1,0:T(8,128)S(1)} all-gather(f32[8,128]{1,0:T(8,128)S(1)} %exp.52), channel_id=2, replica_groups=mesh['sp'=8,'tp'=4] {'sp'}, dimensions={0}, use_global_device_ids=true | all-gather | bytes 36864 | tf_op jit(solution)/shard_map/all_gather | solution.py:14
  103.9 3.8 %exponential_multiply_fusion = f32[8,8,64,128]{3,1,2,0:T(8,128)} fusion(f32[8,8,64,128]{3,1,2,0:T(8,128)} %get-tuple-element.376, f32[8,8,128]{2,1,0:T(8,128)S(1)} %fusion.47, f32[8,64,8,128]{3,2,1,0:T(8,128)S(1)} %bitcast.176), kind=kLoop, calls=%fused_computation.67 | loop fusion | flops 3670016 | bytes 6324224 | tf_op jit(solution)/shard_map/mul | solution.py:121
  107.7 37.2 %all-gather.10.cloned.1.call-done = f32[64,128,128]{2,1,0:T(8,128)} async-done(((f32[8,128,128]{2,1,0:T(8,128)}), f32[64,128,128]{2,1,0:T(8,128)}) %all-gather.10.cloned.1.call-update) | async-done | bytes 4194320 | tf_op jit(solution)/shard_map/all_gather | solution.py:14
  144.9 11.4 %while.28 = (s32[]{:T(128)}, f32[8,128,128]{2,1,0:T(8,128)S(1)}, s32[]{:T(128)}, f32[8,8,128]{2,1,0:T(8,128)S(1)}, f32[8,8,128,128]{3,2,1,0:T(8,128)}, /*index=5*/s32[]{:T(128)}, s32[]{:T(128)}) while((s32[]{:T(128)}, f32[8,128,128]{2,1,0:T(8,128)S(1)}, s32[]{:T(128)}, f32[8,8,128]{2,1,0:T(8,128)S(1)}, ...), condition=%wide.region_5.6_spmd.clone, body=%wide.region_4.5_spmd.clone.sunk | while | flops 524292 | bytes 1585265 | solution.py:26
  144.9 1.4 fusion.75
  146.3 1.4 fusion.75
  147.8 1.4 fusion.75
  149.2 1.4 fusion.75
  150.6 1.4 fusion.75
  152.0 1.4 fusion.75
  153.5 1.4 fusion.75
  154.9 1.4 fusion.75
  156.3 4.7 %multiply_reduce_fusion = (f32[8,64,8]{1,0,2:T(8,128)S(1)}, f32[8,64,8,128]{3,1,0,2:T(8,128)S(1)}) fusion(f32[8,8,64,128]{3,2,0,1:T(8,128)} %get-tuple-element.137, f32[8,8,64,128]{3,1,2,0:T(8,128)} %exponential_multiply_fusion, f32[8,128,128]{2,1,0:T(8,128)S(1)} %get-tuple-element.139), kind=kOutput, calls=%fused_computation.66 | convolution fusion | flops 806875136 | bytes 6832128 | tf_op jit(solution)/shard_map/nhtd,hde->nhte/dot_general | solution.py:122
  161.1 1.2 copy.32
  163.5 2.2 fusion.43
  166.6 32.4 %all-gather.6.cloned.1.call-done = bf16[512,4096]{1,0:T(8,128)(2,1)} async-done(((bf16[512,1024]{1,0:T(8,128)(2,1)}), bf16[512,4096]{1,0:T(8,128)(2,1)}) %all-gather.6.cloned.1.call-update) | async-done | bytes 4194320 | tf_op jit(solution)/shard_map/all_gather | solution.py:127
  199.0 126.6 %all-gather.8.cloned.1.call-done = bf16[4096,1024]{1,0:T(8,128)(2,1)} async-done(((bf16[512,1024]{1,0:T(8,128)(2,1)}), bf16[4096,1024]{1,0:T(8,128)(2,1)}) %all-gather.8.cloned.1.call-update) | async-done | bytes 8388624 | tf_op jit(solution)/shard_map/all_gather | solution.py:94
  325.6 9.1 %convolution_convert_fusion = bf16[512,1024]{1,0:T(8,128)(2,1)S(1)} fusion(bf16[512,4096]{1,0:T(8,128)(2,1)} %all-gather.6.cloned.1.call-done, bf16[4096,1024]{1,0:T(8,128)(2,1)} %all-gather.8.cloned.1.call-done), kind=kOutput, calls=%fused_computation.74 | convolution fusion | flops 4295491584 | bytes 13631488 | tf_op jit(solution)/shard_map/dot_general | solution.py:128
  335.0 5.9 %psum.7 = f32[512]{0:T(512)S(1)} all-reduce(f32[512]{0:T(512)S(1)} %fusion.25), channel_id=1, replica_groups=mesh['sp'=8,'tp'=4] {'tp'}, use_global_device_ids=true, to_apply=%region_9.10 | all-reduce | flops 512 | bytes 4096 | tf_op jit(solution)/shard_map/psum | solution.py:130
  340.9 1.4 fusion.28
  (108 shorter events, 29.8 us)
Async XLA Ops:
  6.5 8.1 %copy-start = (f32[4096]{0:T(1024)S(1)}, f32[4096]{0:T(1024)}, u32[]{:S(2)}) copy-start(f32[4096]{0:T(1024)} %param.18) | copy-start | bytes 49156
  6.5 138.4 %all-gather.10.cloned.1.call-start = ((), (), s32[]{:S(2)}) async-start(), calls=%async_computation.2 | async-start | bytes 4718592 | tf_op jit(solution)/shard_map/all_gather | solution.py:14
  9.2 1.8 copy-start.3
  11.2 1.2 copy-start.4
  14.6 4.0 %copy-start.2 = (f32[64,8,8,128]{3,2,1,0:T(8,128)S(1)}, f32[64,8,8,128]{3,2,1,0:T(8,128)}, u32[]{:S(2)}) copy-start(f32[64,8,8,128]{3,2,1,0:T(8,128)} %copy.48) | copy-start | bytes 6291460
  21.1 81.9 %copy-start.7 = (f32[128]{0:T(128)S(1)}, f32[128]{0:T(128)}, u32[]{:S(2)}) copy-start(f32[128]{0:T(128)} %param.20) | copy-start | bytes 1540
  68.2 0.8 copy-start.1
  69.0 129.9 %all-gather.6.cloned.1.call-start = ((), (), s32[]{:S(2)}) async-start(), calls=%async_computation | async-start | bytes 5242880 | tf_op jit(solution)/shard_map/all_gather | solution.py:127
  162.3 1.2 copy-start.6
  165.8 159.8 %all-gather.8.cloned.1.call-start = ((), (), s32[]{:S(2)}) async-start(), calls=%async_computation.1 | async-start | bytes 9437184 | tf_op jit(solution)/shard_map/all_gather | solution.py:94
  166.5 174.3 %copy-start.5 = (bf16[512,1024]{1,0:T(8,128)(2,1)S(1)}, bf16[512,1024]{1,0:T(8,128)(2,1)}, u32[]{:S(2)}) copy-start(bf16[512,1024]{1,0:T(8,128)(2,1)} %param.23) | copy-start | bytes 3145732
  166.6 174.3 %dynamic-slice-start = ((f32[4096]{0:T(1024)}, s32[]{:T(128)}), f32[1024]{0:T(1024)S(1)}, s32[]{:S(2)}) async-start(f32[4096]{0:T(1024)} %param.22, s32[]{:T(128)} %select_n.32), calls=%async_computation.3 | async-start | bytes 8704 | tf_op jit(solution)/shard_map/dynamic_slice | solution.py:133
Sparse Core Ops, SparseCore 0:
  69.2 75.6 all-gather.9
  165.9 32.9 all-gather.5
  201.1 124.4 all-gather.7
where the time goes:
time: 350 us; the launch traced here: 349 us
  waiting for transfers between devices  197 us (56%)
  matrix products  42.7 us (12%)
  blocking collectives  39 us (11%)
  other arithmetic  29.2 us (8%)
  local copies, waits for them, and re-layouts  26.9 us (8%)
  between operations  13.3 us (4%)
    all_gather x1, waiting for transfers between devices, per_device(): whole_weight = lax.all_gather(output_matrix, 'sp', axis=0, tiled=True)  127 us
    all_gather x1, waiting for transfers between devices, prefix(): everything = jax.tree.map(lambda part: lax.all_gather(part, axis), shard)  37.2 us
    all_gather x1, blocking collectives, prefix(): everything = jax.tree.map(lambda part: lax.all_gather(part, axis), shard)  33.1 us
    all_gather x1, waiting for transfers between devices, per_device(): all_heads = lax.all_gather(mixed_rows, 'tp', axis=1, tiled=True)  32.4 us
    dynamic_slice x24, local copies, waits for them, and re-layouts, per_device(): lax.scan(step_forward, starting_state, (queries, to_blocks(keys_in), to_b...  17.5 us
    select_n x8, other arithmetic, step(): return jax.tree.map(lambda a, b: jnp.where(reached, a, b), new, before)  11 us
    dot_general x8, matrix products, block_update(): jnp.einsum('hsd,hse->hde', keys_in * jnp.exp(ending - running), values_in...  9.24 us
    dot_general x1, matrix products, per_device(): jnp.dot(all_heads, whole_weight, preferred_element_type=jnp.float32)  9.14 us
  transfers between devices with their start and end apart: 3, of which 3 were waited for; matrix products, arithmetic and copies ran while one was open for 2% of the time, Pallas kernels for 0%

commit v1 on v0

--- a/solution.py
+++ b/solution.py
@@ -124,7 +124,14 @@
     )
     heads_out = heads_out.transpose(0, 2, 1, 3).reshape(row_count, head_count, HEAD_DIM)
     mixed_rows = gated_norm(heads_out, output_gate_logits, head_norm_gain)
-    all_heads = lax.all_gather(mixed_rows, "tp", axis=1, tiled=True)
+    count = lax.axis_size("tp")
+    route = [(i, (i + 1) % count) for i in range(count)]
+    terms = [mixed_rows]
+    for stride in range(1, count):
+        terms = [lax.ppermute(terms[0], "tp", route), *terms]
+    full = jnp.concatenate(terms, axis=1)
+    shift = (lax.axis_index("tp") + 1) * terms[-1].shape[1]
+    all_heads = jnp.roll(full, shift, axis=1)
     projected = jnp.dot(all_heads, whole_weight, preferred_element_type=jnp.float32)
     branch = lax.optimization_barrier(projected.astype(jnp.bfloat16)).astype(jnp.float32)
     squares = lax.psum(jnp.sum(branch * branch, axis=1), "tp")

time: 350 us -> 294 us (0.84)
  waiting for transfers between devices: 197 us -> 130 us
  local copies, waits for them, and re-layouts: 26.9 us -> 38.9 us
    all_gather x1, waiting for transfers between devices: 127 us -> 49.5 us  [per_device(): whole_weight = lax.all_gather(output_matrix, 'sp', axis=0, tiled=True)]
    ppermute x0 -> x3, waiting for transfers between devices: none -> 42.8 us  [per_device(): terms = [lax.ppermute(terms[0], 'tp', route), *terms]]
    all_gather x1 -> x0, waiting for transfers between devices: 32.4 us -> none  [per_device(): all_heads = lax.all_gather(mixed_rows, 'tp', axis=1, tiled=True)]
    unnamed x19 -> x32, local copies, waits for them, and re-layouts: 4.89 us -> 15 us
  transfers between devices with their start and end apart: 3 -> 5, of which waited for: 3 -> 5; matrix products, arithmetic and copies ran while one was open for 2% -> 13% of each run, Pallas kernels for 0% -> 0%
where the time goes in v1:
time: 294 us; the launch traced here: 293 us
  waiting for transfers between devices  130 us (44%)
  matrix products  42.5 us (14%)
  blocking collectives  39 us (13%)
  local copies, waits for them, and re-layouts  38.9 us (13%)
  other arithmetic  28.4 us (10%)
  between operations  13.6 us (5%)
    all_gather x1, waiting for transfers between devices, per_device(): whole_weight = lax.all_gather(output_matrix, 'sp', axis=0, tiled=True)  49.5 us
    ppermute x3, waiting for transfers between devices, per_device(): terms = [lax.ppermute(terms[0], 'tp', route), *terms]  42.8 us
    all_gather x1, waiting for transfers between devices, prefix(): everything = jax.tree.map(lambda part: lax.all_gather(part, axis), shard)  36.7 us
    all_gather x1, blocking collectives, prefix(): everything = jax.tree.map(lambda part: lax.all_gather(part, axis), shard)  33.1 us
    dynamic_slice x24, local copies, waits for them, and re-layouts, per_device(): lax.scan(step_forward, starting_state, (queries, to_blocks(keys_in), to_b...  17.6 us
    unnamed x32, local copies, waits for them, and re-layouts  15 us
    select_n x8, other arithmetic, step(): return jax.tree.map(lambda a, b: jnp.where(reached, a, b), new, before)  11.3 us
    dot_general x8, matrix products, block_update(): jnp.einsum('hsd,hse->hde', keys_in * jnp.exp(ending - running), values_in...  9.25 us
  transfers between devices with their start and end apart: 5, of which 5 were waited for; matrix products, arithmetic and copies ran while one was open for 13% of the time, Pallas kernels for 0%

profile of v1, /device:TPU:0, one launch (start us, length us, event | category | flops | bytes accessed | tf_op | source)
XLA Modules:
  0.0 292.9 jit_solution(11331765830208278709)
XLA Ops:
  6.5 1.8 divide_bitcast_fusion
  8.4 1.8 copy.48
  12.5 1.5 bitcast_bitcast_fusion
  14.0 3.9 %fusion.38 = f32[8,8,64,128]{3,1,2,0:T(8,128)} fusion(f32[8,64,8]{2,1,0:T(8,128)S(1)} %bitcast.183, f32[8,128]{1,0:T(8,128)S(1)} %dynamic-slice_bitcast_fusion.1, f32[8,64,8,128]{3,2,1,0:T(8,128)} %bitcast.176), kind=kOutput, calls=%fused_computation.62 | output fusion | flops 34603008 | bytes 4214784 | tf_op jit(solution)/shard_map/jit(cumsum)/reduce_window_sum | solution.py:107
  17.9 2.6 fusion.36
  20.5 47.0 %while.27 = (s32[]{:T(128)}, f32[8,128,128]{2,1,0:T(8,128)S(1)}, f32[8,8,64,128]{3,2,0,1:T(8,128)}, f32[8,8,64,128]{3,1,2,0:T(8,128)}, f32[8,8,64,128]{3,1,2,0:T...) while((s32[]{:T(128)}, f32[8,128,128]{2,1,0:T(8,128)S(1)}, ...), condition=%wide.region_2.3_spmd.clone, body=%wide.region_1.2_spmd.clone.sunk | while | flops 303075328 | bytes 7647856 | solution.py:113
  24.1 1.1 fusion.79
  25.2 1.2 convolution_add_fusion.3
  30.0 1.1 fusion.79
  31.1 1.2 convolution_add_fusion.3
  35.9 1.1 fusion.79
  37.0 1.2 convolution_add_fusion.3
  41.7 1.1 fusion.79
  42.9 1.2 convolution_add_fusion.3
  47.6 1.1 fusion.79
  48.7 1.2 convolution_add_fusion.3
  53.5 1.1 fusion.79
  54.6 1.2 convolution_add_fusion.3
  59.3 1.1 fusion.79
  60.5 1.2 convolution_add_fusion.3
  65.2 1.1 fusion.79
  66.3 1.2 convolution_add_fusion.3
  69.9 33.1 %all-gather = f32[64,128]{1,0:T(8,128)S(1)} all-gather(f32[8,128]{1,0:T(8,128)S(1)} %exp.52), channel_id=2, replica_groups=mesh['sp'=8,'tp'=4] {'sp'}, dimensions={0}, use_global_device_ids=true | all-gather | bytes 36864 | tf_op jit(solution)/shard_map/all_gather | solution.py:14
  103.9 3.6 %exponential_multiply_fusion = f32[8,8,64,128]{3,1,2,0:T(8,128)S(1)} fusion(f32[8,8,64,128]{3,1,2,0:T(8,128)} %get-tuple-element.375, f32[8,8,128]{2,1,0:T(8,128)S(1)} %fusion.52, f32[8,64,8,128]{3,2,1,0:T(8,128)} %bitcast.175), kind=kLoop, calls=%fused_computation.69 | loop fusion | flops 3670016 | bytes 6324224 | tf_op jit(solution)/shard_map/mul | solution.py:121
  107.5 36.7 %all-gather.7.cloned.1.call-done = f32[64,128,128]{2,1,0:T(8,128)} async-done(((f32[8,128,128]{2,1,0:T(8,128)}), f32[64,128,128]{2,1,0:T(8,128)}) %all-gather.7.cloned.1.call-update) | async-done | bytes 4194320 | tf_op jit(solution)/shard_map/all_gather | solution.py:14
  144.2 11.6 %while.28 = (s32[]{:T(128)}, f32[8,128,128]{2,1,0:T(8,128)S(1)}, s32[]{:T(128)}, f32[8,8,128]{2,1,0:T(8,128)S(1)}, f32[8,8,128,128]{3,2,1,0:T(8,128)}, /*index=5*/s32[]{:T(128)}, s32[]{:T(128)}) while((s32[]{:T(128)}, f32[8,128,128]{2,1,0:T(8,128)S(1)}, s32[]{:T(128)}, f32[8,8,128]{2,1,0:T(8,128)S(1)}, ...), condition=%wide.region_5.6_spmd.clone, body=%wide.region_4.5_spmd.clone.sunk | while | flops 524292 | bytes 1585257 | solution.py:26
  144.2 1.4 fusion.80
  145.6 1.4 fusion.80
  147.0 1.4 fusion.80
  148.5 1.4 fusion.80
  149.9 1.4 fusion.80
  151.3 1.4 fusion.80
  152.8 1.5 fusion.80
  154.3 1.5 fusion.80
  155.8 4.7 %multiply_reduce_fusion = (f32[8,64,8]{1,0,2:T(8,128)S(1)}, f32[8,64,8,128]{3,1,0,2:T(8,128)}) fusion(f32[8,8,64,128]{3,2,0,1:T(8,128)} %get-tuple-element.137, f32[8,8,64,128]{3,1,2,0:T(8,128)S(1)} %exponential_multiply_fusion, f32[8,128,128]{2,1,0:T(8,128)S(1)} %get-tuple-element.139), kind=kOutput, calls=%fused_computation.68 | convolution fusion | flops 806875136 | bytes 6832128 | tf_op jit(solution)/shard_map/nhtd,hde->nhte/dot_general | solution.py:122
  160.6 2.8 copy.32
  164.6 1.3 fusion.45
  166.0 14.2 %collective-permute-done = bf16[512,1024]{1,0:T(8,128)(2,1)S(1)} collective-permute-done((bf16[512,1024]{1,0:T(8,128)(2,1)S(1)}, bf16[512,1024]{1,0:T(8,128)(2,1)S(1)}, u32[]{:S(2)}, u32[]{:S(2)}) %collective-permute-start) | collective-permute-done | bytes 1048608 | tf_op jit(solution)/shard_map/ppermute | solution.py:131
  180.2 14.2 %collective-permute-done.1 = bf16[512,1024]{1,0:T(8,128)(2,1)S(1)} collective-permute-done((bf16[512,1024]{1,0:T(8,128)(2,1)S(1)}, bf16[512,1024]{1,0:T(8,128)(2,1)S(1)}, u32[]{:S(2)}, u32[]{:S(2)}) %collective-permute-start.1) | collective-permute-done | bytes 1048608 | tf_op jit(solution)/shard_map/ppermute | solution.py:131
  194.4 14.3 %collective-permute-done.2 = bf16[512,1024]{1,0:T(8,128)(2,1)} collective-permute-done((bf16[512,1024]{1,0:T(8,128)(2,1)S(1)}, bf16[512,1024]{1,0:T(8,128)(2,1)}, u32[]{:S(2)}, u32[]{:S(2)}) %collective-permute-start.2) | collective-permute-done | bytes 1048608 | tf_op jit(solution)/shard_map/ppermute | solution.py:131
  208.7 2.3 constant_dynamic-update-slice_fusion.7
  213.2 1.1 constant_dynamic-update-slice_fusion.4
  214.3 2.3 constant_dynamic-update-slice_fusion.3
  216.6 1.1 constant_dynamic-update-slice_fusion.2
  219.8 49.5 %all-gather.5.cloned.1.call-done = bf16[4096,1024]{1,0:T(8,128)(2,1)} async-done(((bf16[512,1024]{1,0:T(8,128)(2,1)}), bf16[4096,1024]{1,0:T(8,128)(2,1)}) %all-gather.5.cloned.1.call-update) | async-done | bytes 8388624 | tf_op jit(solution)/shard_map/all_gather | solution.py:94
  269.3 9.2 %fusion.49 = bf16[512,1024]{1,0:T(8,128)(2,1)S(1)} fusion(bf16[4096,1024]{1,0:T(8,128)(2,1)} %all-gather.5.cloned.1.call-done, bf16[512,8192]{1,0:T(8,128)(2,1)} %constant_dynamic-update-slice_fusion, s32[]{:T(128)S(6)} %select_n.47), kind=kOutput, calls=%fused_computation.76 | convolution fusion | flops 4295491584 | bytes 13631492 | tf_op jit(solution)/shard_map/dot_general | solution.py:135
  278.8 5.9 %psum.7 = f32[512]{0:T(512)S(1)} all-reduce(f32[512]{0:T(512)S(1)} %fusion.27), channel_id=1, replica_groups=mesh['sp'=8,'tp'=4] {'tp'}, use_global_device_ids=true, to_apply=%region_9.10 | all-reduce | flops 512 | bytes 4096 | tf_op jit(solution)/shard_map/psum | solution.py:137
  284.7 1.4 fusion.30
  (125 shorter events, 39.9 us)
Async XLA Ops:
  6.5 7.4 %copy-start = (f32[4096]{0:T(1024)S(1)}, f32[4096]{0:T(1024)}, u32[]{:S(2)}) copy-start(f32[4096]{0:T(1024)} %param.18) | copy-start | bytes 49156
  6.5 137.6 %all-gather.7.cloned.1.call-start = ((), (), s32[]{:S(2)}) async-start(), calls=%async_computation.1 | async-start | bytes 4718592 | tf_op jit(solution)/shard_map/all_gather | solution.py:14
  8.3 1.8 copy-start.9
  8.3 1.9 copy-start.5
  10.5 1.2 copy-start.6
  11.8 6.2 %copy-start.3 = (f32[64,8,8,128]{3,2,1,0:T(8,128)}, f32[64,8,8,128]{3,2,1,0:T(8,128)S(1)}, u32[]{:S(2)}) copy-start(f32[64,8,8,128]{3,2,1,0:T(8,128)S(1)} %copy.50) | copy-start | bytes 6291460
  14.0 3.9 %copy-start.4 = (f32[64,8,8,128]{3,2,1,0:T(8,128)S(1)}, f32[64,8,8,128]{3,2,1,0:T(8,128)}, u32[]{:S(2)}) copy-start(f32[64,8,8,128]{3,2,1,0:T(8,128)} %copy.48) | copy-start | bytes 6291460
  20.5 82.5 %copy-start.10 = (f32[128]{0:T(128)S(1)}, f32[128]{0:T(128)}, u32[]{:S(2)}) copy-start(f32[128]{0:T(128)} %param.20) | copy-start | bytes 1540
  67.5 0.8 copy-start.2
  68.3 201.0 %all-gather.5.cloned.1.call-start = ((), (), s32[]{:S(2)}) async-start(), calls=%async_computation | async-start | bytes 9437184 | tf_op jit(solution)/shard_map/all_gather | solution.py:94
  163.4 1.2 copy-start.8
  165.9 14.3 %collective-permute-start = (bf16[512,1024]{1,0:T(8,128)(2,1)S(1)}, bf16[512,1024]{1,0:T(8,128)(2,1)S(1)}, u32[]{:S(2)}, u32[]{:S(2)}) collective-permute-start(bf16[512,1024]{1,0:T(8,128)(2,1)S(1)} %fusion.45), channel_id=1, source_target_pairs={{0,1},{1,2},{2,3},{3,0},{4,5},{5,6},{6,7},{7,4},{8,9},{9,10},{10,1... | collective-permute-start | bytes 3145736 | tf_op jit(solution)/shard_map/ppermute | solution.py:131
  180.2 14.2 %collective-permute-start.1 = (bf16[512,1024]{1,0:T(8,128)(2,1)S(1)}, bf16[512,1024]{1,0:T(8,128)(2,1)S(1)}, u32[]{:S(2)}, u32[]{:S(2)}) collective-permute-start(bf16[512,1024]{1,0:T(8,128)(2,1)S(1)} %collective-permute-done), channel_id=1, source_target_pairs={{0,1},{1,2},{2,3},{3,0},{4,5},{5,6},{6,7},{7,4},{8,9},{9,10},{10,1... | collective-permute-start | bytes 3145736 | tf_op jit(solution)/shard_map/ppermute | solution.py:131
  194.4 14.3 %collective-permute-start.2 = (bf16[512,1024]{1,0:T(8,128)(2,1)S(1)}, bf16[512,1024]{1,0:T(8,128)(2,1)}, u32[]{:S(2)}, u32[]{:S(2)}) collective-permute-start(bf16[512,1024]{1,0:T(8,128)(2,1)S(1)} %collective-permute-done.1), channel_id=1, source_target_pairs={{0,1},{1,2},{2,3},{3,0},{4,5},{5,6},{6,7},{7,4},{8,9},{9,10},{10,1... | collective-permute-start | bytes 3145736 | tf_op jit(solution)/shard_map/ppermute | solution.py:131
  219.8 64.8 %copy-start.7 = (bf16[512,1024]{1,0:T(8,128)(2,1)S(1)}, bf16[512,1024]{1,0:T(8,128)(2,1)}, u32[]{:S(2)}) copy-start(bf16[512,1024]{1,0:T(8,128)(2,1)} %param.23) | copy-start | bytes 3145732
  219.8 64.8 %dynamic-slice-start = ((f32[4096]{0:T(1024)}, s32[]{:T(128)}), f32[1024]{0:T(1024)S(1)}, s32[]{:S(2)}) async-start(f32[4096]{0:T(1024)} %param.22, s32[]{:T(128)} %select_n.45), calls=%async_computation.2 | async-start | bytes 8704 | tf_op jit(solution)/shard_map/dynamic_slice | solution.py:140
  269.3 16.7 %copy-start.1 = (f32[4096]{0:T(1024)S(1)}, f32[4096]{0:T(1024)}, u32[]{:S(2)}) copy-start(f32[4096]{0:T(1024)} %param.18) | copy-start | bytes 49156
Sparse Core Ops, SparseCore 0:
  68.4 75.6 all-gather.6
  146.3 122.9 all-gather.4
